TPU v7x, 32 devices: a whole 2x2x4 slice. The times are simulated.
32 devices in a mesh: grp: 2 (over y), fs: 4 (over z), tp: 4 (over x, core).
Axes of the slice: x: 2, y: 2, z: 4, core: 2. Of those that a mesh axis runs over, the one named last changes fastest.
Arguments:
- tokens: bfloat16 [4096, 2048], P(('grp', 'fs', 'tp')), parts along dimension 0, may hold values from -6 to 6
- up_master: float32 [2048, 4096], P('fs', 'tp'), may hold values from -0.125 to 0.125
- down_master: float32 [4096, 2048], P('fs', 'tp'), may hold values from -0.09375 to 0.09375
- norm_gain: float32 [2048], P('fs'), may hold values from 0.1 to 1.9
Outputs:
- up_weights: bfloat16 [4096, 4096], P('grp', 'tp'), parts along dimension 0
- down_weights: bfloat16 [8192, 2048], P(('grp', 'tp')), parts along dimension 0
- mlp_output: bfloat16 [4096, 2048], P(('grp', 'fs', 'tp')), parts along dimension 0
There are 2 independent parts, one for each index of `grp`. A program takes and returns all parts, laid end to end along the dimension named above; an argument that names none is the same for every part. Nothing has to cross between parts.
All inputs are finite; a program needn't handle non-finite values.
Results may differ from a plain program's by a relative error of at most 0.014.
Values may be sent and summed in bfloat16 or wider, within the bound.
A program may use at most 64 MiB of HBM per device.

v0:
```python
import jax
import jax.numpy as jnp
from jax import lax
from jax.sharding import PartitionSpec as P


def on_device(tokens, up_master, down_master, norm_gain):
    up_local = (norm_gain[:, None] * up_master).astype(jnp.bfloat16)
    down_local = down_master.astype(jnp.bfloat16)
    float_tokens = tokens.astype(jnp.float32)
    scale = lax.rsqrt(jnp.mean(float_tokens * float_tokens, axis=-1, keepdims=True) + 1e-06)
    normed_local = (float_tokens * scale).astype(jnp.bfloat16)
    normed = lax.all_gather(normed_local, "tp", axis=0, tiled=True)
    up_weights = lax.all_gather(up_local, "fs", axis=0, tiled=True)
    preact = jnp.dot(normed, up_weights, preferred_element_type=jnp.float32)
    gathered_rows = lax.all_gather(down_local, "fs", axis=0, tiled=True)
    down_weights = lax.all_to_all(gathered_rows, "tp", split_axis=0, concat_axis=1, tiled=True)
    rectified = jax.nn.relu(preact)
    hidden = (rectified * rectified).astype(jnp.bfloat16)
    mlp_output = lax.psum_scatter(
        jnp.dot(hidden, down_weights, preferred_element_type=jnp.float32).astype(jnp.bfloat16),
        "tp",
        scatter_dimension=0,
        tiled=True,
    )
    return (up_weights, down_weights, mlp_output)


def solution(mesh):
    in_specs = (P(("grp", "fs", "tp"), None), P("fs", "tp"), P("fs", "tp"), P("fs"))
    out_specs = (P("grp", "tp"), P(("grp", "tp"), None), P(("grp", "fs", "tp"), None))
    return jax.shard_map(
        on_device, mesh=mesh, in_specs=in_specs, out_specs=out_specs, check_vma=False
    )
```

profile of v0, /device:TPU:0, one launch (start us, length us, event | category | flops | bytes accessed | tf_op | source)
XLA Modules:
  0.0 262.0 jit_solution(9083774294734147993)
XLA Ops:
  7.2 0.0 copy-start.1
  7.2 0.0 all-gather.6.cloned.1.call-start
  7.2 2.7 %convert_element_type.19 = bf16[1024,512]{1,0:T(8,128)(2,1)} convert(f32[1024,512]{1,0:T(8,128)} %param.6) | non-fusion elementwise | flops 524288 | bytes 3145728 | tf_op jit(solution)/shard_map/convert_element_type | solution.py:9
  10.0 0.0 copy-start
  10.0 0.0 copy-start.2
  10.0 0.0 all-gather.6.cloned.1.call-update
  10.0 0.0 all-gather.8.cloned.1.call-start
  10.0 0.0 copy-done.1
  10.1 0.2 fusion
  10.2 1.0 fusion.1
  11.2 0.0 all-gather.8.cloned.1.call-update
  11.2 0.0 all-gather.4.cloned.1.call-start
  11.3 0.5 copy-done
  11.7 0.0 copy-done.2
  11.7 1.1 multiply_convert_fusion.1
  12.9 0.0 all-gather.4.cloned.1.call-update
  12.9 0.0 reduce-scatter.2.cloned.1.call-start
  13.0 80.7 %all-gather.6.cloned.1.call-done = bf16[4096,512]{1,0:T(8,128)(2,1)} async-done(((bf16[1024,512]{1,0:T(8,128)(2,1)}), bf16[4096,512]{1,0:T(8,128)(2,1)}) %all-gather.6.cloned.1.call-update) | async-done | bytes 4194320 | tf_op jit(solution)/shard_map/all_gather | solution.py:16
  93.6 65.1 %all_to_all.19 = bf16[4,1024,512]{2,1,0:T(8,128)(2,1)} all-to-all(bf16[4,1024,512]{2,1,0:T(8,128)(2,1)} %bitcast.9), channel_id=1, replica_groups=mesh['grp'=2,'fs'=4,'tp'=4] {'tp'}, dimensions={0} | all-to-all | bytes 8388608 | tf_op jit(solution)/shard_map/all_to_all | solution.py:17
  158.7 6.2 %copy.8 = bf16[4,1024,512]{1,2,0:T(8,128)(2,1)} copy(bf16[4,1024,512]{2,1,0:T(8,128)(2,1)} %all_to_all.19) | data formatting | bytes 8388608 | tf_op jit(solution)/shard_map/all_to_all | solution.py:17
  164.9 0.0 all-gather.8.cloned.1.call-done
  164.9 46.2 %all-gather.4.cloned.1.call-done = bf16[2048,1024]{1,0:T(8,128)(2,1)} async-done(((bf16[512,1024]{1,0:T(8,128)(2,1)}), bf16[2048,1024]{1,0:T(8,128)(2,1)}) %all-gather.4.cloned.1.call-update) | async-done | bytes 4194320 | tf_op jit(solution)/shard_map/all_gather | solution.py:14
  211.1 9.9 %convolution_convert_fusion = bf16[512,2048]{1,0:T(8,128)(2,1)} fusion(bf16[1024,2048]{0,1:T(8,128)(2,1)} %bitcast.7, bf16[512,2048]{1,0:T(8,128)(2,1)} %all-gather.8.cloned.1.call-done, bf16[2048,1024]{1,0:T(8,128)(2,1)} %all-gather.4.cloned.1.call-done), kind=kOutput, calls=%fused_computation | convolution fusion | flops 4297588736 | bytes 12582912 | tf_op jit(solution)/shard_map/dot_general | solution.py:21
  221.0 0.0 reduce-scatter.2.cloned.1.call-update
  221.0 6.4 %copy.9 = bf16[1024,2048]{1,0:T(8,128)(2,1)} copy(bf16[1024,2048]{0,1:T(8,128)(2,1)} %bitcast.8) | data formatting | bytes 8388608
  227.4 23.4 %reduce-scatter.2.cloned.1.call-done = bf16[128,2048]{1,0:T(8,128)(2,1)} async-done(((bf16[512,2048]{1,0:T(8,128)(2,1)}), bf16[128,2048]{1,0:T(8,128)(2,1)}) %reduce-scatter.2.cloned.1.call-update) | async-done | bytes 524304 | tf_op jit(solution)/shard_map/reduce_scatter | solution.py:20
  250.8 4.6 %copy.11 = bf16[2048,1024]{1,0:T(8,128)(2,1)} copy(bf16[2048,1024]{1,0:T(8,128)(2,1)} %all-gather.4.cloned.1.call-done) | data formatting | bytes 8388608
  (1 shorter events, 0.0 us)
Async XLA Ops:
  7.2 2.9 %copy-start.1 = (bf16[128,2048]{1,0:T(8,128)(2,1)S(1)}, bf16[128,2048]{1,0:T(8,128)(2,1)}, u32[]{:S(2)}) copy-start(bf16[128,2048]{1,0:T(8,128)(2,1)} %param.4) | copy-start | bytes 1572868
  7.2 86.4 %all-gather.6.cloned.1.call-start = ((), (), s32[]{:S(2)}) async-start(), calls=%async_computation.3 | async-start | bytes 5242880 | tf_op jit(solution)/shard_map/all_gather | solution.py:16
  10.0 1.8 copy-start
  10.0 1.8 copy-start.2
  10.0 154.9 %all-gather.8.cloned.1.call-start = ((), (), s32[]{:S(2)}) async-start(), calls=%async_computation.4 | async-start | bytes 2621440 | tf_op jit(solution)/shard_map/all_gather | solution.py:13
  11.2 199.9 %all-gather.4.cloned.1.call-start = ((), (), s32[]{:S(2)}) async-start(), calls=%async_computation.2 | async-start | bytes 5242880 | tf_op jit(solution)/shard_map/all_gather | solution.py:14
  12.9 237.9 %reduce-scatter.2.cloned.1.call-start = ((), (), s32[]{:S(2)}) async-start(), calls=%async_computation.5 | async-start | bytes 2621440 | tf_op jit(solution)/shard_map/reduce_scatter | solution.py:20
Sparse Core Ops, SparseCore 0:
  10.1 83.4 all-gather.5
  95.8 32.3 all-gather.7
  130.3 80.7 all-gather.3
  221.1 29.6 reduce-scatter.1
where the time goes:
time: 263 us; the launch traced here: 262 us
  waiting for transfers between devices  150 us (57%)
  blocking collectives  65.1 us (25%)
  local copies, waits for them, and re-layouts  17.8 us (7%)
  between operations  13.8 us (5%)
  matrix products  9.89 us (4%)
  other arithmetic  5.04 us (2%)
    all_gather x1, waiting for transfers between devices, on_device(): gathered_rows = lax.all_gather(down_local, 'fs', axis=0, tiled=True)  80.7 us
    all_to_all x1, blocking collectives, on_device(): lax.all_to_all(gathered_rows, 'tp', split_axis=0, concat_axis=1, tiled=True)  65.1 us
    all_gather x1, waiting for transfers between devices, on_device(): up_weights = lax.all_gather(up_local, 'fs', axis=0, tiled=True)  46.2 us
    reduce_scatter x1, waiting for transfers between devices, on_device(): lax.psum_scatter(jnp.dot(hidden, down_weights, preferred_element_type=jnp...  23.4 us
    unnamed x8, local copies, waits for them, and re-layouts  11.5 us
    dot_general x1, matrix products, on_device(): jnp.dot(hidden, down_weights, preferred_element_type=jnp.float32)  9.89 us
    all_to_all x1, local copies, waits for them, and re-layouts, on_device(): lax.all_to_all(gathered_rows, 'tp', split_axis=0, concat_axis=1, tiled=True)  6.21 us
  transfers between devices with their start and end apart: 4, of which 3 were waited for; matrix products, arithmetic and copies ran while one was open for 6% of the time, Pallas kernels for 0%

commit v1 on v0

--- a/solution.py
+++ b/solution.py
@@ -11,7 +11,12 @@
     scale = lax.rsqrt(jnp.mean(float_tokens * float_tokens, axis=-1, keepdims=True) + 1e-06)
     normed_local = (float_tokens * scale).astype(jnp.bfloat16)
     normed = lax.all_gather(normed_local, "tp", axis=0, tiled=True)
-    up_weights = lax.all_gather(up_local, "fs", axis=0, tiled=True)
+    ring = [up_local]
+    for hop in range(3):
+        ring.append(lax.ppermute(ring[-1], "fs", [(dev, (dev + 1) % 4) for dev in range(4)]))
+    up_weights = jnp.roll(
+        jnp.concatenate(ring[::-1], axis=0), (lax.axis_index("fs") + 1) * ring[0].shape[0], axis=0
+    )
     preact = jnp.dot(normed, up_weights, preferred_element_type=jnp.float32)
     gathered_rows = lax.all_gather(down_local, "fs", axis=0, tiled=True)
     down_weights = lax.all_to_all(gathered_rows, "tp", split_axis=0, concat_axis=1, tiled=True)

time: 263 us -> 247 us (0.939)
  blocking collectives: 65.1 us -> 0 us
  starting transfers between devices: 0.16 us -> 22.5 us
  waiting for transfers between devices: 150 us -> 171 us
  local copies, waits for them, and re-layouts: 17.8 us -> 20.7 us
    ppermute x0 -> x3, waiting for transfers between devices: none -> 66.4 us  [on_device(): lax.ppermute(ring[-1], 'fs', [(dev, (dev + 1) % 4) for dev in range(4)])]
    all_to_all x1 -> x0, blocking collectives: 65.1 us -> none  [on_device(): lax.all_to_all(gathered_rows, 'tp', split_axis=0, concat_axis=1, tiled=True)]
    all_gather x1 -> x0, waiting for transfers between devices: 46.2 us -> none  [on_device(): up_weights = lax.all_gather(up_local, 'fs', axis=0, tiled=True)]
    all_to_all x0 -> x1, waiting for transfers between devices: none -> 21.5 us  [on_device(): lax.all_to_all(gathered_rows, 'tp', split_axis=0, concat_axis=1, tiled=True)]
    all_gather x1, waiting for transfers between devices: 80.7 us -> 61.1 us  [on_device(): gathered_rows = lax.all_gather(down_local, 'fs', axis=0, tiled=True)]
    ppermute x0 -> x3, starting transfers between devices: none -> 17.5 us  [on_device(): lax.ppermute(ring[-1], 'fs', [(dev, (dev + 1) % 4) for dev in range(4)])]
    all_to_all x0 -> x1, starting transfers between devices: none -> 4.84 us  [on_device(): lax.all_to_all(gathered_rows, 'tp', split_axis=0, concat_axis=1, tiled=True)]
    unnamed x8 -> x11, local copies, waits for them, and re-layouts: 11.5 us -> 11.9 us
  transfers between devices with their start and end apart: 4 -> 7, of which waited for: 3 -> 5; matrix products, arithmetic and copies ran while one was open for 6% -> 10% of each run, Pallas kernels for 0% -> 0%
where the time goes in v1:
time: 247 us; the launch traced here: 246 us
  waiting for transfers between devices  171 us (69%)
  starting transfers between devices  22.5 us (9%)
  local copies, waits for them, and re-layouts  20.7 us (8%)
  between operations  15.6 us (6%)
  matrix products  9.9 us (4%)
  other arithmetic  6.58 us (3%)
    ppermute x3, waiting for transfers between devices, on_device(): lax.ppermute(ring[-1], 'fs', [(dev, (dev + 1) % 4) for dev in range(4)])  66.4 us
    all_gather x1, waiting for transfers between devices, on_device(): gathered_rows = lax.all_gather(down_local, 'fs', axis=0, tiled=True)  61.1 us
    reduce_scatter x1, waiting for transfers between devices, on_device(): lax.psum_scatter(jnp.dot(hidden, down_weights, preferred_element_type=jnp...  22.1 us
    all_to_all x1, waiting for transfers between devices, on_device(): lax.all_to_all(gathered_rows, 'tp', split_axis=0, concat_axis=1, tiled=True)  21.5 us
    ppermute x3, starting transfers between devices, on_device(): lax.ppermute(ring[-1], 'fs', [(dev, (dev + 1) % 4) for dev in range(4)])  17.5 us
    unnamed x11, local copies, waits for them, and re-layouts  11.9 us
    dot_general x1, matrix products, on_device(): jnp.dot(hidden, down_weights, preferred_element_type=jnp.float32)  9.9 us
    all_to_all x1, local copies, waits for them, and re-layouts, on_device(): lax.all_to_all(gathered_rows, 'tp', split_axis=0, concat_axis=1, tiled=True)  6.31 us
  transfers between devices with their start and end apart: 7, of which 5 were waited for; matrix products, arithmetic and copies ran while one was open for 10% of the time, Pallas kernels for 0%

profile of v1, /device:TPU:0, one launch (start us, length us, event | category | flops | bytes accessed | tf_op | source)
XLA Modules:
  0.0 246.4 jit_solution(6121737993728472597)
XLA Ops:
  8.0 0.0 copy-start
  8.0 0.0 copy-start.1
  8.0 0.0 all-gather.3.cloned.1.call-start
  8.1 2.8 %convert_element_type.19 = bf16[1024,512]{1,0:T(8,128)(2,1)} convert(f32[1024,512]{1,0:T(8,128)} %param.6) | non-fusion elementwise | flops 524288 | bytes 3145728 | tf_op jit(solution)/shard_map/convert_element_type | solution.py:9
  10.9 0.0 all-gather.3.cloned.1.call-update
  10.9 0.0 copy-done
  10.9 0.0 copy-done.1
  10.9 0.2 multiply_convert_fusion.1
  11.1 3.1 %collective-permute-start = (bf16[512,1024]{1,0:T(8,128)(2,1)S(1)}, bf16[512,1024]{1,0:T(8,128)(2,1)S(1)}, u32[]{:S(2)}, u32[]{:S(2)}) collective-permute-start(bf16[512,1024]{1,0:T(8,128)(2,1)S(1)} %multiply_convert_fusion.1), channel_id=1, source_target_pairs={{0,4},{4,8},{8,12},{12,0},{1,5},{5,9},{9,13},{13,1},{2,6},{6,10},{... | collective-permute-start | bytes 3145736 | tf_op jit(solution)/shard_map/ppermute | solution.py:16
  14.2 38.9 %collective-permute-done = bf16[512,1024]{1,0:T(8,128)(2,1)S(1)} collective-permute-done((bf16[512,1024]{1,0:T(8,128)(2,1)S(1)}, bf16[512,1024]{1,0:T(8,128)(2,1)S(1)}, u32[]{:S(2)}, u32[]{:S(2)}) %collective-permute-start) | collective-permute-done | bytes 1048608 | tf_op jit(solution)/shard_map/ppermute | solution.py:16
  53.1 14.3 %collective-permute-start.1 = (bf16[512,1024]{1,0:T(8,128)(2,1)S(1)}, bf16[512,1024]{1,0:T(8,128)(2,1)}, u32[]{:S(2)}, u32[]{:S(2)}) collective-permute-start(bf16[512,1024]{1,0:T(8,128)(2,1)S(1)} %collective-permute-done), channel_id=1, source_target_pairs={{0,4},{4,8},{8,12},{12,0},{1,5},{5,9},{9,13},{13,1},{2,6},{6,10},{... | collective-permute-start | bytes 3145736 | tf_op jit(solution)/shard_map/ppermute | solution.py:16
  67.4 1.2 fusion
  68.7 61.1 %all-gather.3.cloned.1.call-done = bf16[4096,512]{1,0:T(8,128)(2,1)} async-done(((bf16[1024,512]{1,0:T(8,128)(2,1)}), bf16[4096,512]{1,0:T(8,128)(2,1)}) %all-gather.3.cloned.1.call-update) | async-done | bytes 4194320 | tf_op jit(solution)/shard_map/all_gather | solution.py:21
  129.8 4.8 %all-to-all-start = ((bf16[4,1024,512]{2,1,0:T(8,128)(2,1)}), bf16[4,1024,512]{2,1,0:T(8,128)(2,1)}, u32[]{:S(2)}, u32[]{:S(2)}) async-start(bf16[4,1024,512]{2,1,0:T(8,128)(2,1)} %bitcast.9), calls=%async_computation | async-start | bytes 8388608 | tf_op jit(solution)/shard_map/all_to_all | solution.py:22
  134.7 0.0 all-gather.5.cloned.1.call-start
  134.7 2.0 fusion.1
  136.7 0.0 all-gather.5.cloned.1.call-update
  136.7 0.0 reduce-scatter.2.cloned.1.call-start
  136.8 0.0 collective-permute-done.1
  136.8 0.1 collective-permute-start.2
  136.9 27.6 %collective-permute-done.2 = bf16[512,1024]{1,0:T(8,128)(2,1)} collective-permute-done((bf16[512,1024]{1,0:T(8,128)(2,1)}, bf16[512,1024]{1,0:T(8,128)(2,1)}, u32[]{:S(2)}, u32[]{:S(2)}) %collective-permute-start.2) | collective-permute-done | bytes 1048608 | tf_op jit(solution)/shard_map/ppermute | solution.py:16
  164.4 1.3 constant_dynamic-update-slice_fusion.7
  165.7 1.3 constant_dynamic-update-slice_fusion.6
  167.0 0.1 constant_dynamic-update-slice_fusion.5
  167.1 0.2 constant_dynamic-update-slice_fusion.4
  167.3 1.3 constant_dynamic-update-slice_fusion.3
  168.6 1.3 constant_dynamic-update-slice_fusion.2
  169.9 0.1 constant_dynamic-update-slice_fusion.1
  170.0 0.2 constant_dynamic-update-slice_fusion
  170.2 2.5 constant_dynamic-slice_fusion
  172.6 21.5 %all-to-all-done = bf16[4,1024,512]{2,1,0:T(8,128)(2,1)} async-done(((bf16[4,1024,512]{2,1,0:T(8,128)(2,1)}), bf16[4,1024,512]{2,1,0:T(8,128)(2,1)}, u32[]{:S(2)}, u32[]{:S(2)}) %all-to-all-start) | async-done | bytes 4194336 | tf_op jit(solution)/shard_map/all_to_all | solution.py:22
  194.1 6.3 %copy.8 = bf16[4,1024,512]{1,2,0:T(8,128)(2,1)} copy(bf16[4,1024,512]{2,1,0:T(8,128)(2,1)} %all-to-all-done) | data formatting | bytes 8388608 | tf_op jit(solution)/shard_map/all_to_all | solution.py:22
  200.4 0.0 all-gather.5.cloned.1.call-done
  200.4 9.9 %convolution_convert_fusion = bf16[512,2048]{1,0:T(8,128)(2,1)} fusion(bf16[1024,2048]{0,1:T(8,128)(2,1)} %bitcast.7, bf16[512,2048]{1,0:T(8,128)(2,1)} %all-gather.5.cloned.1.call-done, bf16[2048,1024]{1,0:T(8,128)(2,1)} %constant_dynamic-slice_fusion), kind=kOutput, calls=%fused_computation | convolution fusion | flops 4297588736 | bytes 12582912 | tf_op jit(solution)/shard_map/dot_general | solution.py:26
  210.3 0.0 reduce-scatter.2.cloned.1.call-update
  210.3 6.5 %copy.9 = bf16[1024,2048]{1,0:T(8,128)(2,1)} copy(bf16[1024,2048]{0,1:T(8,128)(2,1)} %bitcast.8) | data formatting | bytes 8388608
  216.9 22.1 %reduce-scatter.2.cloned.1.call-done = bf16[128,2048]{1,0:T(8,128)(2,1)} async-done(((bf16[512,2048]{1,0:T(8,128)(2,1)}), bf16[128,2048]{1,0:T(8,128)(2,1)}) %reduce-scatter.2.cloned.1.call-update) | async-done | bytes 524304 | tf_op jit(solution)/shard_map/reduce_scatter | solution.py:25
  (1 shorter events, 0.0 us)
Async XLA Ops:
  8.0 2.9 %copy-start = (f32[512,1024]{1,0:T(8,128)S(1)}, f32[512,1024]{1,0:T(8,128)}, u32[]{:S(2)}) copy-start(f32[512,1024]{1,0:T(8,128)} %param.5) | copy-start | bytes 6291460
  8.0 2.9 %copy-start.1 = (f32[512]{0:T(512)S(1)}, f32[512]{0:T(512)}, u32[]{:S(2)}) copy-start(f32[512]{0:T(512)} %param.7) | copy-start | bytes 6148
  8.0 121.8 %all-gather.3.cloned.1.call-start = ((), (), s32[]{:S(2)}) async-start(), calls=%async_computation.2 | async-start | bytes 5242880 | tf_op jit(solution)/shard_map/all_gather | solution.py:21
  11.1 42.0 %collective-permute-start = (bf16[512,1024]{1,0:T(8,128)(2,1)S(1)}, bf16[512,1024]{1,0:T(8,128)(2,1)S(1)}, u32[]{:S(2)}, u32[]{:S(2)}) collective-permute-start(bf16[512,1024]{1,0:T(8,128)(2,1)S(1)} %multiply_convert_fusion.1), channel_id=1, source_target_pairs={{0,4},{4,8},{8,12},{12,0},{1,5},{5,9},{9,13},{13,1},{2,6},{6,10},{... | collective-permute-start | bytes 3145736 | tf_op jit(solution)/shard_map/ppermute | solution.py:16
  53.1 83.7 %collective-permute-start.1 = (bf16[512,1024]{1,0:T(8,128)(2,1)S(1)}, bf16[512,1024]{1,0:T(8,128)(2,1)}, u32[]{:S(2)}, u32[]{:S(2)}) collective-permute-start(bf16[512,1024]{1,0:T(8,128)(2,1)S(1)} %collective-permute-done), channel_id=1, source_target_pairs={{0,4},{4,8},{8,12},{12,0},{1,5},{5,9},{9,13},{13,1},{2,6},{6,10},{... | collective-permute-start | bytes 3145736 | tf_op jit(solution)/shard_map/ppermute | solution.py:16
  129.8 64.3 %all-to-all-start = ((bf16[4,1024,512]{2,1,0:T(8,128)(2,1)}), bf16[4,1024,512]{2,1,0:T(8,128)(2,1)}, u32[]{:S(2)}, u32[]{:S(2)}) async-start(bf16[4,1024,512]{2,1,0:T(8,128)(2,1)} %bitcast.9), calls=%async_computation | async-start | bytes 8388608 | tf_op jit(solution)/shard_map/all_to_all | solution.py:22
  134.7 65.8 %all-gather.5.cloned.1.call-start = ((), (), s32[]{:S(2)}) async-start(), calls=%async_computation.3 | async-start | bytes 2621440 | tf_op jit(solution)/shard_map/all_gather | solution.py:13
  136.7 102.2 %reduce-scatter.2.cloned.1.call-start = ((), (), s32[]{:S(2)}) async-start(), calls=%async_computation.4 | async-start | bytes 2621440 | tf_op jit(solution)/shard_map/reduce_scatter | solution.py:25
  136.8 27.6 %collective-permute-start.2 = (bf16[512,1024]{1,0:T(8,128)(2,1)}, bf16[512,1024]{1,0:T(8,128)(2,1)}, u32[]{:S(2)}, u32[]{:S(2)}) collective-permute-start(bf16[512,1024]{1,0:T(8,128)(2,1)} %collective-permute-done.1), channel_id=1, source_target_pairs={{0,4},{4,8},{8,12},{12,0},{1,5},{5,9},{9,13},{13,1},{2,6},{6,10},{... | collective-permute-start | bytes 3145736 | tf_op jit(solution)/shard_map/ppermute | solution.py:16
Sparse Core Ops, SparseCore 0:
  11.0 118.7 all-gather.2
Sparse Core Ops, SparseCore 1:
  137.3 32.6 all-gather.4
  210.4 28.5 reduce-scatter.1
